TPU v7x, 512 devices: a 8x2x16 block of a 8x8x16 slice. The times are simulated.
512 devices in a mesh: grp: 2 (over y), sp: 32 (over z, core), tp: 8 (over x).
Axes of the slice: x: 8, y: 2, z: 16, core: 2. Of those that a mesh axis runs over, the one named last changes fastest.
The devices are a block of a 8x8x16 slice.
Arguments:
- prompt_rows: bfloat16 [49152, 2048], P(('grp', 'sp')), parts along dimension 0, may hold values from -6 to 6
- norm_gain: float32 [2048], replicated, may hold values from 0.1 to 1.9
- key_weight: bfloat16 [2048, 1024], P(None, 'tp'), may hold values from -0.125 to 0.125
- value_weight: bfloat16 [2048, 1024], P(None, 'tp'), may hold values from -0.125 to 0.125
- new_query: bfloat16 [2048], P(('grp', 'tp')), parts along dimension 0, may hold values from -6 to 6
- score_offset: float32 [16], P('tp'), may hold values from -11.5 to -4
- output_gain: float32 [1024], P('tp'), may hold values from 0.1 to 1.9
Outputs:
- key_cache: bfloat16 [16, 32, 32, 48, 64], P(('grp', 'tp'), 'sp'), parts along dimension 0
- value_cache: bfloat16 [16, 32, 32, 48, 64], P(('grp', 'tp'), 'sp'), parts along dimension 0
- first_read: bfloat16 [2048], P(('grp', 'tp')), parts along dimension 0
There are 2 independent parts, one for each index of `grp`. A program takes and returns all parts, laid end to end along the dimension named above; an argument that names none is the same for every part. Nothing has to cross between parts.
All inputs are finite; a program needn't handle non-finite values.
Results may differ from a plain program's by a relative error of at most 0.0059.
Values may be sent and summed in bfloat16 or wider, within the bound.
No kernel may reach another device: no remote copies, remote signals or barrier semaphores. Data moves between devices by JAX's collectives and lax.ppermute only.
A program may use at most 64 MiB of HBM per device.

v0:
```python
import jax
import jax.numpy as jnp
from jax import lax
from jax.sharding import PartitionSpec as P

EPSILON = 1e-06


def side_by_side(arrays, axis, split_dim, concat_dim, along):
    both = jnp.concatenate(arrays, axis=along)
    result, at, done = (
        lax.all_to_all(both, axis, split_axis=split_dim, concat_axis=concat_dim, tiled=True),
        0,
        [],
    )
    for a in arrays:
        done.append(lax.slice_in_dim(result, at, at + a.shape[along], axis=along))
        at += a.shape[along]
    return tuple(done)


def copy_for_each(value, axis):
    copies = jnp.broadcast_to(value, (lax.axis_size(axis), *value.shape))
    return lax.all_to_all(copies, axis, split_axis=0, concat_axis=0, tiled=True)


def folded_in_pairs(pieces, combine):
    while len(jax.tree.leaves(pieces)[0]) > 1:
        pieces = jax.vmap(combine)(*(pieces[side::2] for side in (0, 1)))
    return pieces[0]


def carried_in(value, axis, combine, identity):
    peers, position = (lax.axis_size(axis), lax.axis_index(axis))
    passed = jnp.arange(peers) > position

    def kept(part, zero, own):
        part = jnp.where(
            passed.reshape(-1, *(1 for _ in own.shape)), part, jnp.asarray(zero, own.dtype)
        )
        return part[::-1]

    pieces = copy_for_each(value, axis)
    return folded_in_pairs(kept(pieces, identity, value), combine)


def taken_together(value, axis):
    everything = copy_for_each(value, axis)
    return jnp.sum(everything, axis=0)


def normalize(rows, norm_gain):
    rows32 = rows.astype(jnp.float32)
    mean_square = jnp.mean(rows32 * rows32, axis=-1, keepdims=True)
    return (rows32 * lax.rsqrt(mean_square + EPSILON) * norm_gain).astype(jnp.bfloat16)


def project_rows(rows, norm_gain, key_weight, value_weight):
    normed = normalize(rows, norm_gain)
    keys = jnp.dot(normed, key_weight, preferred_element_type=jnp.float32).astype(jnp.bfloat16)
    values = jnp.dot(normed, value_weight, preferred_element_type=jnp.float32).astype(jnp.bfloat16)
    return (keys, values)


def cache_layout(keys, values, head_count):
    devices = lax.axis_size("sp")
    subs = devices // head_count
    depth = keys.shape[1] // head_count
    rows = keys.shape[0] // subs

    def arrange(cache):
        split = cache.reshape(subs, rows, head_count, depth)
        return jnp.transpose(split, (2, 0, 1, 3)).reshape(devices, 1, rows, depth)

    moved_keys, moved_values = side_by_side((arrange(keys), arrange(values)), "sp", 0, 1, 2)
    target = (1, 1, devices, rows, depth)
    return (moved_keys.reshape(target), moved_values.reshape(target))


def add_terms(first_part, second_part):
    return first_part + second_part


def read_early(new_query, keys, values, score_offset):
    head_count = score_offset.shape[0]
    depth = keys.shape[1] // head_count
    query2 = new_query.reshape(head_count, depth)
    keys3 = keys.reshape(keys.shape[0], head_count, depth)
    scores = jnp.einsum("hd,shd->hs", query2, keys3, preferred_element_type=jnp.float32)
    scores = scores * depth ** (-0.5) + score_offset[:, None]
    remain = jax.nn.log_sigmoid(-scores)
    within = lax.cumsum(remain, axis=1, reverse=True) - remain
    totals = jnp.sum(remain, axis=1)
    beyond = carried_in(totals, "sp", add_terms, jnp.zeros_like(totals))
    sticks = jnp.exp(jax.nn.log_sigmoid(scores) + within + beyond[:, None]).astype(jnp.bfloat16)
    values3 = values.reshape(values.shape[0], head_count, depth)
    partial_value = jnp.einsum("hs,shd->hd", sticks, values3, preferred_element_type=jnp.float32)
    return taken_together(partial_value, "sp")


def finish_read(mixed, output_gain, head_count):
    spread = jnp.mean(mixed * mixed, axis=-1, keepdims=True)
    result = mixed * lax.rsqrt(spread + EPSILON) * output_gain.reshape(head_count, -1)
    return result.reshape(-1).astype(jnp.bfloat16)


def body(prompt_rows, norm_gain, key_weight, value_weight, new_query, score_offset, output_gain):
    head_count = score_offset.shape[0]
    keys_here, values_here = project_rows(prompt_rows, norm_gain, key_weight, value_weight)
    keys_all, values_all = cache_layout(keys_here, values_here, head_count)
    local_keys, local_values = project_rows(prompt_rows, norm_gain, key_weight, value_weight)
    mixed = read_early(new_query, local_keys, local_values, score_offset)
    return (keys_all, values_all, finish_read(mixed, output_gain, head_count))


def solution(mesh):
    in_specs = (
        P(("grp", "sp"), None),
        P(),
        P(None, "tp"),
        P(None, "tp"),
        P(("grp", "tp")),
        P("tp"),
        P("tp"),
    )
    out_specs = (
        P(("grp", "tp"), "sp", None, None, None),
        P(("grp", "tp"), "sp", None, None, None),
        P(("grp", "tp")),
    )
    return jax.shard_map(body, mesh=mesh, in_specs=in_specs, out_specs=out_specs, check_vma=False)
```

profile of v0, /device:TPU:65, one launch (start us, length us, event | category | flops | bytes accessed | tf_op | source)
XLA Modules:
  0.0 125.6 jit_solution(13984382602272751206)
XLA Ops:
  0.7 0.8 reshape.95
  1.5 2.7 %fusion = f32[768]{0:T(1024)S(1)} fusion(bf16[768,2048]{1,0:T(8,128)(2,1)} %param.7), kind=kLoop, calls=%fused_computation.2 | loop fusion | flops 4717824 | bytes 3148800 | tf_op jit(solution)/shard_map/reduce_sum | solution.py:54
  4.3 1.3 %convolution_convert_fusion.1 = bf16[768,128]{0,1:T(8,128)(2,1)S(1)} fusion(bf16[2048,128]{1,0:T(8,128)(2,1)S(1)} %copy-done, bf16[768,2048]{1,0:T(8,128)(2,1)S(1)} %copy-done.1, f32[2048]{0:T(1024)S(1)} %copy-done.4, f32[768]{0:T(1024)S(1)} %add_rsqrt_fusion), kind=kOutput, calls=%fused_computation.6 | convolution fusion | flops 409042944 | bytes 3877888 | tf_op jit(solution)/shard_map/dot_general | solution.py:60
  6.0 0.6 broadcast_in_dim.25
  6.6 45.2 %all-to-all-start.1 = ((f32[32,1,2]{2,1,0:T(1,128)}), f32[32,1,2]{2,1,0:T(1,128)S(1)}, u32[]{:S(2)}, u32[]{:S(2)}) async-start(f32[32,1,2]{2,1,0:T(1,128)} %broadcast_in_dim.25), calls=%async_computation.1 | async-start | bytes 32768 | tf_op jit(solution)/shard_map/all_to_all | solution.py:24
  51.8 3.2 %convolution_convert_fusion = bf16[768,128]{0,1:T(8,128)(2,1)S(1)} fusion(bf16[2048,128]{1,0:T(8,128)(2,1)S(1)} %copy-done.3, bf16[768,2048]{1,0:T(8,128)(2,1)} %param.7, f32[2048]{0:T(1024)S(1)} %copy-done.4, f32[768]{0:T(1024)S(1)} %add_rsqrt_fusion), kind=kOutput, calls=%fused_computation.5 | convolution fusion | flops 409042944 | bytes 3877888 | tf_op jit(solution)/shard_map/dot_general | solution.py:61
  55.0 2.5 %reduce-window.6 = f32[2,6,128]{2,1,0:T(8,128)S(1)} reduce-window(f32[2,6,128]{2,1,0:T(8,128)S(1)} %reshape.87, f32[]{:T(128)} %constant.8.clone.1), window={size=1x1x128 pad=0_0x0_0x0_127}, to_apply=%region_1.0 | reduce-window | flops 195072 | bytes 12292 | tf_op jit(solution)/shard_map/reduce-window
  57.6 0.2 reduce-window.9
  58.1 0.2 reshape.79
  58.6 0.2 reshape.81
  58.8 4.8 %all-to-all-done.1 = f32[32,1,2]{2,1,0:T(1,128)S(1)} async-done(((f32[32,1,2]{2,1,0:T(1,128)}), f32[32,1,2]{2,1,0:T(1,128)S(1)}, u32[]{:S(2)}, u32[]{:S(2)}) %all-to-all-start.1) | async-done | bytes 288 | tf_op jit(solution)/shard_map/all_to_all | solution.py:24
  64.7 0.2 add_reduce_fusion
  65.2 0.7 reshape.98
  65.9 7.9 %all-to-all-start.2 = ((f32[32,1,128]{2,1,0:T(1,128)}), f32[32,1,128]{2,1,0:T(1,128)S(1)}, u32[]{:S(2)}, u32[]{:S(2)}) async-start(f32[32,1,128]{2,1,0:T(1,128)} %reshape.98), calls=%async_computation.2 | async-start | bytes 32768 | tf_op jit(solution)/shard_map/all_to_all | solution.py:24
  74.0 1.1 copy.38
  75.0 10.3 %all-to-all-done.2 = f32[32,1,128]{2,1,0:T(1,128)S(1)} async-done(((f32[32,1,128]{2,1,0:T(1,128)}), f32[32,1,128]{2,1,0:T(1,128)S(1)}, u32[]{:S(2)}, u32[]{:S(2)}) %all-to-all-start.2) | async-done | bytes 16416 | tf_op jit(solution)/shard_map/all_to_all | solution.py:24
  85.3 4.7 %all-to-all-start = ((bf16[32,1,96,64]{2,3,1,0:T(8,128)(2,1)}), bf16[32,1,96,64]{2,3,1,0:T(8,128)(2,1)S(1)}, u32[]{:S(2)}, u32[]{:S(2)}) async-start(bf16[32,1,96,64]{2,3,1,0:T(8,128)(2,1)} %copy.38), calls=%async_computation | async-start | bytes 1048576 | tf_op jit(solution)/shard_map/all_to_all | solution.py:12
  90.0 0.5 broadcast.62
  90.5 0.7 reduce.4
  91.6 0.5 multiply_convert_fusion
  92.2 31.3 %all-to-all-done = bf16[32,1,96,64]{2,3,1,0:T(8,128)(2,1)S(1)} async-done(((bf16[32,1,96,64]{2,3,1,0:T(8,128)(2,1)}), bf16[32,1,96,64]{2,3,1,0:T(8,128)(2,1)S(1)}, u32[]{:S(2)}, u32[]{:S(2)}) %all-to-all-start) | async-done | bytes 393248 | tf_op jit(solution)/shard_map/all_to_all | solution.py:12
  123.4 0.2 slice_bitcast_fusion
  123.7 1.0 copy.42
  124.6 1.0 copy.41
  (52 shorter events, 3.1 us)
Async XLA Ops:
  0.6 3.6 %copy-start = (bf16[2048,128]{1,0:T(8,128)(2,1)S(1)}, bf16[2048,128]{1,0:T(8,128)(2,1)}, u32[]{:S(2)}) copy-start(bf16[2048,128]{1,0:T(8,128)(2,1)} %param.9) | copy-start | bytes 1572868
  0.6 3.6 %copy-start.4 = (f32[2048]{0:T(1024)S(1)}, f32[2048]{0:T(1024)}, u32[]{:S(2)}) copy-start(f32[2048]{0:T(1024)} %param.8) | copy-start | bytes 24580
  1.4 2.9 %copy-start.1 = (bf16[768,2048]{1,0:T(8,128)(2,1)S(1)}, bf16[768,2048]{1,0:T(8,128)(2,1)}, u32[]{:S(2)}) copy-start(bf16[768,2048]{1,0:T(8,128)(2,1)} %param.7) | copy-start | bytes 9437188
  4.3 1.5 %copy-start.2 = (f32[2]{0:T(128)S(1)}, f32[2]{0:T(128)}, u32[]{:S(2)}) copy-start(f32[2]{0:T(128)} %param.12) | copy-start | bytes 28
  4.3 47.5 %copy-start.3 = (bf16[2048,128]{1,0:T(8,128)(2,1)S(1)}, bf16[2048,128]{1,0:T(8,128)(2,1)}, u32[]{:S(2)}) copy-start(bf16[2048,128]{1,0:T(8,128)(2,1)} %param.10) | copy-start | bytes 1572868
  6.6 57.0 %all-to-all-start.1 = ((f32[32,1,2]{2,1,0:T(1,128)}), f32[32,1,2]{2,1,0:T(1,128)S(1)}, u32[]{:S(2)}, u32[]{:S(2)}) async-start(f32[32,1,2]{2,1,0:T(1,128)} %broadcast_in_dim.25), calls=%async_computation.1 | async-start | bytes 32768 | tf_op jit(solution)/shard_map/all_to_all | solution.py:24
  58.4 33.3 %copy-start.5 = (f32[128]{0:T(128)S(1)}, f32[128]{0:T(128)}, u32[]{:S(2)}) copy-start(f32[128]{0:T(128)} %param.13) | copy-start | bytes 1540
  65.9 19.4 %all-to-all-start.2 = ((f32[32,1,128]{2,1,0:T(1,128)}), f32[32,1,128]{2,1,0:T(1,128)S(1)}, u32[]{:S(2)}, u32[]{:S(2)}) async-start(f32[32,1,128]{2,1,0:T(1,128)} %reshape.98), calls=%async_computation.2 | async-start | bytes 32768 | tf_op jit(solution)/shard_map/all_to_all | solution.py:24
  85.3 38.1 %all-to-all-start = ((bf16[32,1,96,64]{2,3,1,0:T(8,128)(2,1)}), bf16[32,1,96,64]{2,3,1,0:T(8,128)(2,1)S(1)}, u32[]{:S(2)}, u32[]{:S(2)}) async-start(bf16[32,1,96,64]{2,3,1,0:T(8,128)(2,1)} %copy.38), calls=%async_computation | async-start | bytes 1048576 | tf_op jit(solution)/shard_map/all_to_all | solution.py:12
where the time goes:
time: 126 us
  starting transfers between devices  57.8 us (46%)
  waiting for transfers between devices  46.4 us (37%)
  local copies, waits for them, and re-layouts  8.21 us (7%)
  other arithmetic  7.65 us (6%)
  matrix products  4.78 us (4%)
    all_to_all x2, starting transfers between devices, copy_for_each(): return lax.all_to_all(copies, axis, split_axis=0, concat_axis=0, tiled=True)  53 us
    all_to_all x1, waiting for transfers between devices, side_by_side(): lax.all_to_all(both, axis, split_axis=split_dim, concat_axis=concat_dim,...  31.3 us
    all_to_all x2, waiting for transfers between devices, copy_for_each(): return lax.all_to_all(copies, axis, split_axis=0, concat_axis=0, tiled=True)  15.1 us
    all_to_all x1, starting transfers between devices, side_by_side(): lax.all_to_all(both, axis, split_axis=split_dim, concat_axis=concat_dim,...  4.71 us
    dot_general x1, matrix products, project_rows(): jnp.dot(normed, value_weight, preferred_element_type=jnp.float32)  3.18 us
    unnamed x16, local copies, waits for them, and re-layouts  2.85 us
    reduce_sum x1, other arithmetic, normalize(): mean_square = jnp.mean(rows32 * rows32, axis=-1, keepdims=True)  2.72 us
    another operation x2, other arithmetic  2.68 us
  transfers between devices with their start and end apart: 3, of which 3 were waited for; matrix products, arithmetic and copies ran while one was open for 8% of the time, Pallas kernels for 0%

commit v1 on v0

v1 whole, which is shorter than its diff:
```python
import jax
import jax.numpy as jnp
from jax import lax
from jax.experimental import pallas as pl
from jax.experimental.pallas import tpu as pltpu
from jax.sharding import PartitionSpec as P

EPSILON = 1e-06
HIGHEST = lax.Precision.HIGHEST
EXTRA = 8
STEPS = 4


def split3(value):
    high = value.astype(jnp.bfloat16).astype(jnp.float32)
    rest = value - high
    middle = rest.astype(jnp.bfloat16).astype(jnp.float32)
    return high, middle, rest - middle


def fill_kernel(
    x_hbm, gain_ref, kw_hbm, vw_hbm, query_ref, offset_ref, out_ref, x_ref, w_ref, x_sem, w_sem
):
    steps, tile, _ = x_ref.shape
    columns = kw_hbm.shape[1]
    half = columns // 2
    rows = out_ref.shape[3] - EXTRA
    pairs = tile // rows // 2

    key_copy = pltpu.make_async_copy(kw_hbm, w_ref.at[:, pl.ds(0, columns)], w_sem.at[0])
    value_copy = pltpu.make_async_copy(vw_hbm, w_ref.at[:, pl.ds(columns, columns)], w_sem.at[1])
    copies = [
        pltpu.make_async_copy(x_hbm.at[pl.ds(i * tile, tile), :], x_ref.at[i], x_sem.at[i])
        for i in range(steps)
    ]
    copies[steps - 1].start()
    key_copy.start()
    value_copy.start()
    for i in reversed(range(steps - 1)):
        copies[i].start()

    low = lax.broadcasted_iota(jnp.int32, (tile, columns), 1) < half
    low8 = lax.broadcasted_iota(jnp.int32, (8, columns), 1) < half
    query = query_ref[...].astype(jnp.float32)
    queries = [
        jnp.where(low8, query, 0.0).astype(jnp.bfloat16),
        jnp.where(low8, pltpu.roll(query, half, 1), 0.0).astype(jnp.bfloat16),
    ]
    upper = (
        lax.broadcasted_iota(jnp.int32, (tile, tile), 0)
        > lax.broadcasted_iota(jnp.int32, (tile, tile), 1)
    ).astype(jnp.float32)
    later = [jnp.zeros((8, 1), jnp.float32) for _ in range(2)]
    mixed = [jnp.zeros((8, columns), jnp.float32) for _ in range(2)]
    for i in reversed(range(steps)):
        copies[i].wait()
        x32 = x_ref[i].astype(jnp.float32)
        mean_square = jnp.mean(x32 * x32, axis=-1, keepdims=True)
        normed = (x32 * lax.rsqrt(mean_square + EPSILON) * gain_ref[...]).astype(jnp.bfloat16)
        if i == steps - 1:
            key_copy.wait()
            value_copy.wait()
        both = jnp.dot(normed, w_ref[...], preferred_element_type=jnp.float32)
        keys, values = both[:, :columns], both[:, columns:]
        heads = [
            jnp.where(low, keys, pltpu.roll(values, half, 1)).astype(jnp.bfloat16),
            jnp.where(low, pltpu.roll(keys, half, 1), values).astype(jnp.bfloat16),
        ]
        for h in range(2):
            head = heads[h]
            for j in range(2 * pairs):
                out_ref[j % 2, h, i * pairs + j // 2, 0:rows, :] = head[j * rows : (j + 1) * rows]
            scores = lax.dot_general(
                queries[h], head, (((1,), (1,)), ((), ())), preferred_element_type=jnp.float32
            )
            scores = scores * half ** (-0.5) + offset_ref[h]
            soft = jnp.log1p(jnp.exp(-jnp.abs(scores)))
            remain = -(jnp.maximum(scores, 0.0) + soft)
            taken = jnp.minimum(scores, 0.0) - soft
            within = jnp.dot(remain, upper, precision=HIGHEST, preferred_element_type=jnp.float32)
            sticks = jnp.exp(taken + within + later[h])
            rounded = sticks.astype(jnp.bfloat16)
            rest = (sticks - rounded.astype(jnp.float32)).astype(jnp.bfloat16)
            mixed[h] = mixed[h] + jnp.dot(rounded, head, preferred_element_type=jnp.float32)
            mixed[h] = mixed[h] + jnp.dot(rest, head, preferred_element_type=jnp.float32)
            later[h] = later[h] + jnp.sum(remain, axis=1, keepdims=True)

    line = lax.broadcasted_iota(jnp.int32, (8, columns), 0)
    lane = lax.broadcasted_iota(jnp.int32, (8, columns), 1)
    weighted = jnp.where(low8, pltpu.roll(mixed[0], half, 1), mixed[1])
    high = weighted.astype(jnp.bfloat16).astype(jnp.float32)
    sums = jnp.zeros((8, columns), jnp.float32)
    for at, part in enumerate(split3(later[0]) + split3(later[1])):
        sums = jnp.where(lane == at, part, sums)
    payload = jnp.where(line == 0, high, jnp.where(line == 1, weighted - high, 0.0))
    payload = jnp.where(line == 2, sums, payload).astype(jnp.bfloat16)
    shape = (*out_ref.shape[:3], EXTRA, columns)
    out_ref[:, :, :, rows:, :] = jnp.broadcast_to(payload, shape)


def fill(rows, norm_gain, key_weight, value_weight, query, offset, subs):
    count, width = rows.shape
    columns = key_weight.shape[1]
    sub_rows = count // subs
    heads = offset.shape[0]
    tile = count // STEPS
    vmem = pl.BlockSpec(memory_space=pltpu.VMEM)
    hbm = pl.BlockSpec(memory_space=pl.ANY)
    return pl.pallas_call(
        fill_kernel,
        in_specs=[hbm, vmem, hbm, hbm, vmem, pl.BlockSpec(memory_space=pltpu.SMEM)],
        out_specs=vmem,
        out_shape=jax.ShapeDtypeStruct((2, heads, subs // 2, sub_rows + EXTRA, columns), jnp.bfloat16),
        scratch_shapes=[
            pltpu.VMEM((STEPS, tile, width), jnp.bfloat16),
            pltpu.VMEM((width, 2 * columns), jnp.bfloat16),
            pltpu.SemaphoreType.DMA((STEPS,)),
            pltpu.SemaphoreType.DMA((2,)),
        ],
        name="fill",
    )(rows, norm_gain.reshape(1, width), key_weight, value_weight, query, offset)


def settle_kernel(moved_ref, gain_ref, keys_ref, values_ref, read_ref):
    peers, rows, half = moved_ref.shape[0], keys_ref.shape[2], keys_ref.shape[3]
    columns = 2 * half
    chips = peers // 2
    for c in range(2):
        both = moved_ref[c * chips : (c + 1) * chips, 0:rows, :]
        keys_ref[:, c] = both[:, :, :half]
        values_ref[:, c] = both[:, :, half:]

    payload = moved_ref[:, rows:, :].astype(jnp.float32)
    line = lax.broadcasted_iota(jnp.int32, payload.shape, 1)
    weighted = jnp.sum(jnp.where(line < 2, payload, 0.0), axis=1)
    sums = jnp.sum(jnp.where(line == 2, payload, 0.0), axis=1)
    at_row = lax.broadcasted_iota(jnp.int32, (peers, peers), 0)
    at_col = lax.broadcasted_iota(jnp.int32, (peers, peers), 1)
    block_row = lax.rem(at_row, chips) * 2 + at_row // chips
    block_col = lax.rem(at_col, chips) * 2 + at_col // chips
    after = (block_col > block_row).astype(jnp.float32)
    beyond = jnp.dot(after, sums, precision=HIGHEST, preferred_element_type=jnp.float32)
    lane = lax.broadcasted_iota(jnp.int32, (peers, columns), 1)
    first = jnp.sum(jnp.where(lane < 3, beyond, 0.0), axis=1, keepdims=True)
    second = jnp.sum(jnp.where((lane >= 3) & (lane < 6), beyond, 0.0), axis=1, keepdims=True)
    low = lane < half
    mixed = jnp.sum(weighted * jnp.exp(jnp.where(low, first, second)), axis=0, keepdims=True)
    low = low[0:1]
    square = mixed * mixed
    first = jnp.sum(jnp.where(low, square, 0.0), axis=1, keepdims=True) / half
    second = jnp.sum(jnp.where(low, 0.0, square), axis=1, keepdims=True) / half
    scale = lax.rsqrt(jnp.where(low, first, second) + EPSILON)
    read_ref[...] = (mixed * scale * gain_ref[...]).astype(jnp.bfloat16)


def settle(moved, gain):
    peers, rows, columns = moved.shape
    rows = rows - EXTRA
    cache = jax.ShapeDtypeStruct((peers // 2, 2, rows, columns // 2), jnp.bfloat16)
    vmem = pl.BlockSpec(memory_space=pltpu.VMEM)
    return pl.pallas_call(
        settle_kernel,
        in_specs=[vmem, vmem],
        out_specs=[vmem, vmem, vmem],
        out_shape=[cache, cache, jax.ShapeDtypeStruct((1, columns), jnp.bfloat16)],
        name="settle",
    )(moved, gain.reshape(1, columns))


def body(prompt_rows, norm_gain, key_weight, value_weight, new_query, score_offset, output_gain):
    heads = score_offset.shape[0]
    peers = lax.axis_size("sp")
    subs = peers // heads
    columns = key_weight.shape[1]
    query = jnp.broadcast_to(new_query.reshape(1, columns), (8, columns))
    packed = fill(prompt_rows, norm_gain, key_weight, value_weight, query, score_offset, subs)
    block = packed.shape[3]
    order = [*range(0, peers, 2), *range(1, peers, 2)]
    moved = lax.all_to_all(
        packed.reshape(peers, block, columns), "sp", 0, 0, axis_index_groups=[order], tiled=True
    )
    keys, values, first_read = settle(moved, output_gain)
    target = (1, 1, peers, block - EXTRA, columns // heads)
    return (keys.reshape(target), values.reshape(target), first_read.reshape(columns))


def solution(mesh):
    in_specs = (
        P(("grp", "sp"), None),
        P(),
        P(None, "tp"),
        P(None, "tp"),
        P(("grp", "tp")),
        P("tp"),
        P("tp"),
    )
    out_specs = (
        P(("grp", "tp"), "sp", None, None, None),
        P(("grp", "tp"), "sp", None, None, None),
        P(("grp", "tp")),
    )
    return jax.shard_map(body, mesh=mesh, in_specs=in_specs, out_specs=out_specs, check_vma=False)
```

time: 126 us -> 88.1 us (0.70)
  blocking collectives: 0 us -> 73.9 us
  starting transfers between devices: 57.8 us -> 0 us
  waiting for transfers between devices: 46.4 us -> 0 us
  Pallas kernels: 0 us -> 12.1 us
  other arithmetic: 7.65 us -> 0 us
  local copies, waits for them, and re-layouts: 8.21 us -> 1.23 us
  matrix products: 4.78 us -> 0 us
    all_to_all x0 -> x1, blocking collectives: none -> 73.9 us  [body(): lax.all_to_all(packed.reshape(peers, block, columns), 'sp', 0, 0, axis_in...]
    all_to_all x3 -> x0, starting transfers between devices: 57.8 us -> none  [the longest x2 53 us: copy_for_each(): return lax.all_to_all(copies, axis, split_axis=0, concat_axis=0, tiled=True)]
    all_to_all x3 -> x0, waiting for transfers between devices: 46.4 us -> none  [the longest x1 31.3 us: side_by_side(): lax.all_to_all(both, axis, split_axis=split_dim, concat_axis=concat_dim,...]
    pallas_call x0 -> x2, Pallas kernels: none -> 12.1 us  [the longest x1 9.92 us: fill(): pl.pallas_call(fill_kernel, in_specs=[hbm, vmem, hbm, hbm, vmem, pl.Block...]
    dot_general x4 -> x0, matrix products: 4.78 us -> none  [the longest x1 3.18 us: project_rows(): jnp.dot(normed, value_weight, preferred_element_type=jnp.float32)]
    reduce_sum x4 -> x0, other arithmetic: 3.01 us -> none  [the longest x1 2.72 us: normalize(): mean_square = jnp.mean(rows32 * rows32, axis=-1, keepdims=True)]
    unnamed x16 -> x0, local copies, waits for them, and re-layouts: 2.85 us -> none
    another operation x2 -> x0, other arithmetic: 2.68 us -> none
  transfers between devices with their start and end apart: 3 -> 0, of which waited for: 3 -> 0; matrix products, arithmetic and copies ran while one was open for 8% -> 0% of each run, Pallas kernels for 0% -> 0%
where the time goes in v1:
time: 88.1 us; the launch traced here: 87.8 us
  blocking collectives  73.9 us (84%)
  Pallas kernels  12.1 us (14%)
  local copies, waits for them, and re-layouts  1.23 us (1%)
    all_to_all x1, blocking collectives, body(): lax.all_to_all(packed.reshape(peers, block, columns), 'sp', 0, 0, axis_in...  73.9 us
    pallas_call x1, Pallas kernels, fill(): pl.pallas_call(fill_kernel, in_specs=[hbm, vmem, hbm, hbm, vmem, pl.Block...  9.92 us
    pallas_call x1, Pallas kernels, settle(): pl.pallas_call(settle_kernel, in_specs=[vmem, vmem], out_specs=[vmem, vme...  2.17 us

profile of v1, /device:TPU:65, one launch (start us, length us, event | category | flops | bytes accessed | tf_op | source)
XLA Modules:
  0.0 87.8 jit_solution(12080943691822305938)
XLA Ops:
  0.6 1.2 %broadcast_in_dim.2.query_ref = bf16[8,128]{1,0:T(8,128)(2,1)} broadcast(bf16[128]{0:T(256)(128)(2,1)} %param.11), dimensions={1} | broadcast | bytes 2304 | tf_op jit(solution)/shard_map/broadcast_in_dim | solution.py:175
  1.9 9.9 %fill.1 = bf16[2,2,8,56,128]{4,3,2,1,0:T(8,128)(2,1)} custom-call(bf16[768,2048]{1,0:T(8,128)(2,1)} %x_hbm.1, f32[1,2048]{1,0:T(1,128)} %bitcast.7, bf16[2048,128]{1,0:T(8,128)(2,1)} %kw_hbm.1, bf16[2048,128]{1,0:T(8,128)(2,1)} %vw_hbm.1, bf16[8,128]{1,0:T(8,128)(2,1)} %broadcast_in_dim.2.query_ref, f32[2]{0:T(128)} %offset_ref.1), custom_call_target="tpu_custom_call" | custom-call | tf_op jit(solution)/shard_map/fill/pallas_call | solution.py:109
  11.8 73.9 %all_to_all.5.moved_ref = bf16[32,56,128]{2,1,0:T(8,128)(2,1)} all-to-all(bf16[32,56,128]{2,1,0:T(8,128)(2,1)} %bitcast.6), channel_id=1, replica_groups={{0,16,32,48,64,80,96,112,128,144,160,176,192,208,224,240,8,24,40,56,72,..., dimensions={0} | all-to-all | bytes 917504 | tf_op jit(solution)/shard_map/all_to_all | solution.py:179
  85.7 2.2 %settle.1 = (bf16[16,2,48,64]{3,2,1,0:T(8,128)(2,1)}, bf16[16,2,48,64]{3,2,1,0:T(8,128)(2,1)}, bf16[1,128]{1,0:T(2,128)(2,1)}) custom-call(bf16[32,56,128]{2,1,0:T(8,128)(2,1)} %all_to_all.5.moved_ref, f32[1,128]{1,0:T(1,128)} %bitcast.8), custom_call_target="tpu_custom_call" | custom-call | tf_op jit(solution)/shard_map/settle/pallas_call | solution.py:161

commit v2 on v1

v2 whole, which is shorter than its diff:
```python
import jax
import jax.numpy as jnp
from jax import lax
from jax.experimental import pallas as pl
from jax.experimental.pallas import tpu as pltpu
from jax.sharding import PartitionSpec as P

EPSILON = 1e-06
STEPS = 2
APART = 4
GROUP = 32


def split3(value):
    high = value.astype(jnp.bfloat16).astype(jnp.float32)
    rest = value - high
    middle = rest.astype(jnp.bfloat16).astype(jnp.float32)
    return high, middle, rest - middle


def fill_kernel(
    x_hbm, gain_hbm, kw_hbm, vw_hbm, query_hbm, offset_hbm, out_ref,
    x_ref, w_ref, gain_ref, query_ref, offset_ref, normed_ref, head_ref, x_sem, w_sem, sem,
):
    steps, tile, _ = x_ref.shape
    columns = kw_hbm.shape[1]
    half = columns // 2
    rows = 2 * (out_ref.shape[3] - 1)
    apart, chips = out_ref.shape[1], out_ref.shape[1] * out_ref.shape[2]
    count = steps * tile
    chunks = count // columns

    copies = [
        pltpu.make_async_copy(x_hbm.at[pl.ds(i * tile, tile), :], x_ref.at[i], x_sem.at[i])
        for i in range(steps)
    ]
    gain_copy = pltpu.make_async_copy(gain_hbm, gain_ref, sem.at[0])
    query_copy = pltpu.make_async_copy(query_hbm, query_ref, sem.at[1])
    offset_copy = pltpu.make_async_copy(offset_hbm, offset_ref, sem.at[2])
    key_copy = pltpu.make_async_copy(kw_hbm, w_ref.at[:, pl.ds(0, columns)], w_sem.at[0])
    value_copy = pltpu.make_async_copy(vw_hbm, w_ref.at[:, pl.ds(columns, columns)], w_sem.at[1])
    gain_copy.start()
    key_copy.start()
    value_copy.start()
    copies[0].start()
    for i in range(1, steps):
        copies[i].start(priority=1)
    query_copy.start()
    offset_copy.start()

    low = lax.broadcasted_iota(jnp.int32, (tile, columns), 1) < half

    pairs = tile // rows // 2

    def multiply(i, carry):
        pltpu.make_async_copy(
            x_hbm.at[pl.ds(i * tile, tile), :], x_ref.at[i], x_sem.at[i]
        ).wait()
        for r in range(0, tile, GROUP):
            x32 = x_ref[i, r : r + GROUP, :].astype(jnp.float32)
            mean_square = jnp.mean(x32 * x32, axis=-1, keepdims=True)
            scale = lax.rsqrt(mean_square + EPSILON)
            normed_ref[r : r + GROUP, :] = (x32 * scale * gain_ref[...]).astype(jnp.bfloat16)
        both = jnp.dot(normed_ref[...], w_ref[...], preferred_element_type=jnp.float32)
        keys, values = both[:, :columns], both[:, columns:]
        heads = [
            jnp.where(low, keys, pltpu.roll(values, half, 1)).astype(jnp.bfloat16),
            jnp.where(low, pltpu.roll(keys, half, 1), values).astype(jnp.bfloat16),
        ]
        for h in range(2):
            head_ref[h, pl.ds(i * tile, tile), :] = heads[h]
            for j in range(2 * pairs):
                chip = h * (chips // 2) + i * pairs + j // 2
                out_ref[j % 2, lax.rem(chip, apart), lax.div(chip, apart), 0 : rows // 2] = heads[h][
                    j * rows : (j + 1) * rows
                ].reshape(rows // 2, 2, columns)
        return carry

    gain_copy.wait()
    key_copy.wait()
    value_copy.wait()
    lax.fori_loop(0, steps, multiply, 0)
    query_copy.wait()
    offset_copy.wait()

    low8 = lax.broadcasted_iota(jnp.int32, (8, columns), 1) < half
    query = jnp.broadcast_to(query_ref[...].astype(jnp.float32), (8, columns))
    queries = [
        jnp.where(low8, query, 0.0).astype(jnp.bfloat16),
        jnp.where(low8, pltpu.roll(query, half, 1), 0.0).astype(jnp.bfloat16),
    ]
    upper = (
        lax.broadcasted_iota(jnp.int32, (columns, columns), 0)
        > lax.broadcasted_iota(jnp.int32, (columns, columns), 1)
    ).astype(jnp.bfloat16)
    scores = jnp.concatenate(
        [
            lax.dot_general(
                queries[h], head_ref[h], (((1,), (1,)), ((), ())), preferred_element_type=jnp.float32
            )
            * half ** (-0.5)
            + offset_ref[h]
            for h in range(2)
        ],
        axis=0,
    )
    soft = jnp.log1p(jnp.exp(-jnp.abs(scores)))
    remain = -(jnp.maximum(scores, 0.0) + soft)
    taken = jnp.minimum(scores, 0.0) - soft
    pieces = [remain[:, c * columns : (c + 1) * columns] for c in range(chunks)]
    stacked = jnp.concatenate(
        [part.astype(jnp.bfloat16) for piece in pieces for part in split3(piece)], axis=0
    )
    summed = jnp.dot(stacked, upper, preferred_element_type=jnp.float32)
    later = jnp.zeros((16, 1), jnp.float32)
    after = [None] * chunks
    for c in reversed(range(chunks)):
        base = c * 48
        within = summed[base : base + 16] + summed[base + 16 : base + 32] + summed[base + 32 : base + 48]
        after[c] = within + later
        later = later + jnp.sum(pieces[c], axis=1, keepdims=True)
    sticks = jnp.exp(taken + jnp.concatenate(after, axis=1))
    rounded = sticks.astype(jnp.bfloat16).astype(jnp.float32)
    rest = sticks - rounded
    mixed = []
    for h in range(2):
        parts = jnp.concatenate([rounded[h * 8 : h * 8 + 8], rest[h * 8 : h * 8 + 8]], axis=0)
        products = jnp.dot(
            parts.astype(jnp.bfloat16), head_ref[h], preferred_element_type=jnp.float32
        )
        mixed.append(products[0:8] + products[8:16])

    line = lax.broadcasted_iota(jnp.int32, (8, columns), 0)
    lane = lax.broadcasted_iota(jnp.int32, (8, columns), 1)
    weighted = jnp.where(low8, pltpu.roll(mixed[0], half, 1), mixed[1])
    sums = jnp.zeros((8, columns), jnp.float32)
    for at, part in enumerate(split3(later[0:8]) + split3(later[8:16])):
        sums = jnp.where(lane == at, part, sums)
    payload = jnp.where(line == 0, weighted, sums)[0:2].astype(jnp.bfloat16)
    shape = (*out_ref.shape[:3], 1, 2, columns)
    out_ref[:, :, :, rows // 2 :] = jnp.broadcast_to(payload, shape)


def fill(rows, norm_gain, key_weight, value_weight, query, offset, subs):
    count, width = rows.shape
    columns = key_weight.shape[1]
    sub_rows = count // subs
    heads = offset.shape[0]
    tile = count // STEPS
    hbm = pl.BlockSpec(memory_space=pl.ANY)
    chips = heads * subs // 2
    out_shape = (2, APART, chips // APART, sub_rows // 2 + 1, 2, columns)
    return pl.pallas_call(
        fill_kernel,
        in_specs=[hbm] * 6,
        out_specs=pl.BlockSpec(memory_space=pltpu.VMEM),
        out_shape=pltpu.VMEM(out_shape, jnp.bfloat16),
        scratch_shapes=[
            pltpu.VMEM((STEPS, tile, width), jnp.bfloat16),
            pltpu.VMEM((width, 2 * columns), jnp.bfloat16),
            pltpu.VMEM((1, width), jnp.float32),
            pltpu.VMEM((1, columns), jnp.bfloat16),
            pltpu.SMEM((heads,), jnp.float32),
            pltpu.VMEM((tile, width), jnp.bfloat16),
            pltpu.VMEM((heads, count, columns), jnp.bfloat16),
            pltpu.SemaphoreType.DMA((STEPS,)),
            pltpu.SemaphoreType.DMA((2,)),
            pltpu.SemaphoreType.DMA((3,)),
        ],
        name="fill",
    )(
        rows, norm_gain.reshape(1, width), key_weight, value_weight,
        query.reshape(1, columns), offset,
    )


def block_of(at, chips):
    near = chips // APART
    inside = at % chips
    return (inside % near * APART + inside // near) * 2 + at // chips


def settle_kernel(
    moved_ref, gain_ref, keys_hbm, values_hbm, read_hbm, keys_ref, values_ref, read_ref, sem
):
    peers, rows, half = moved_ref.shape[0], keys_ref.shape[3], keys_ref.shape[4]
    columns = 2 * half
    chips = peers // 2
    copies = []
    near = chips // APART
    for c in range(2):
        both = moved_ref[c * chips : (c + 1) * chips, 0 : rows // 2]
        both = both.reshape(chips, rows, columns)
        for i in range(APART):
            keys_ref[c, :, i] = both[i * near : (i + 1) * near, :, :half]
        copies.append(pltpu.make_async_copy(keys_ref.at[c], keys_hbm.at[:, :, c], sem.at[2 * c]))
        copies[-1].start()
        for i in range(APART):
            values_ref[c, :, i] = both[i * near : (i + 1) * near, :, half:]
        copies.append(
            pltpu.make_async_copy(values_ref.at[c], values_hbm.at[:, :, c], sem.at[2 * c + 1])
        )
        copies[-1].start()

    payload = moved_ref[:, rows // 2].astype(jnp.float32)
    weighted, sums = payload[:, 0, :], payload[:, 1, :]
    at_row = lax.broadcasted_iota(jnp.int32, (peers, peers), 0)
    at_col = lax.broadcasted_iota(jnp.int32, (peers, peers), 1)
    after = (block_of(at_col, chips) > block_of(at_row, chips)).astype(jnp.bfloat16)
    beyond = jnp.dot(after, sums.astype(jnp.bfloat16), preferred_element_type=jnp.float32)
    lane = lax.broadcasted_iota(jnp.int32, (peers, columns), 1)
    first = jnp.sum(jnp.where(lane < 3, beyond, 0.0), axis=1, keepdims=True)
    second = jnp.sum(jnp.where((lane >= 3) & (lane < 6), beyond, 0.0), axis=1, keepdims=True)
    low = lane < half
    mixed = jnp.sum(weighted * jnp.exp(jnp.where(low, first, second)), axis=0, keepdims=True)
    low = low[0:1]
    square = mixed * mixed
    first = jnp.sum(jnp.where(low, square, 0.0), axis=1, keepdims=True) / half
    second = jnp.sum(jnp.where(low, 0.0, square), axis=1, keepdims=True) / half
    scale = lax.rsqrt(jnp.where(low, first, second) + EPSILON)
    read_ref[...] = (mixed * scale * gain_ref[...]).astype(jnp.bfloat16)
    copies.append(pltpu.make_async_copy(read_ref, read_hbm, sem.at[4]))
    copies[-1].start()
    for copy in copies:
        copy.wait()


def settle(moved, gain):
    peers, rows, _, columns = moved.shape
    rows, half = 2 * (rows - 1), columns // 2
    chips = (peers // 2 // APART, APART)
    cache = jax.ShapeDtypeStruct((*chips, 2, rows, half), jnp.bfloat16)
    vmem = pl.BlockSpec(memory_space=pltpu.VMEM)
    hbm = pl.BlockSpec(memory_space=pl.ANY)
    buffer = pltpu.VMEM((2, *chips, rows, half), jnp.bfloat16)
    return pl.pallas_call(
        settle_kernel,
        in_specs=[vmem, vmem],
        out_specs=[hbm, hbm, hbm],
        out_shape=[cache, cache, jax.ShapeDtypeStruct((1, columns), jnp.bfloat16)],
        scratch_shapes=[
            buffer, buffer, pltpu.VMEM((1, columns), jnp.bfloat16), pltpu.SemaphoreType.DMA((5,)),
        ],
        name="settle",
    )(
        pltpu.with_memory_space_constraint(moved, pltpu.VMEM),
        pltpu.with_memory_space_constraint(gain.reshape(1, columns), pltpu.VMEM),
    )


def body(prompt_rows, norm_gain, key_weight, value_weight, new_query, score_offset, output_gain):
    heads = score_offset.shape[0]
    peers = lax.axis_size("sp")
    subs = peers // heads
    columns = key_weight.shape[1]
    packed = fill(prompt_rows, norm_gain, key_weight, value_weight, new_query, score_offset, subs)
    packed = packed.reshape(peers, *packed.shape[3:])
    order = [block_of(at, peers // 2) for at in range(peers)]
    moved = lax.all_to_all(
        packed, "sp", split_axis=0, concat_axis=0, axis_index_groups=[order], tiled=True
    )
    keys, values, first_read = settle(moved, output_gain)
    target = (1, 1, peers, 2 * (packed.shape[1] - 1), columns // heads)
    return (keys.reshape(target), values.reshape(target), first_read.reshape(columns))


def solution(mesh):
    in_specs = (
        P(("grp", "sp"), None),
        P(),
        P(None, "tp"),
        P(None, "tp"),
        P(("grp", "tp")),
        P("tp"),
        P("tp"),
    )
    out_specs = (
        P(("grp", "tp"), "sp", None, None, None),
        P(("grp", "tp"), "sp", None, None, None),
        P(("grp", "tp")),
    )
    return jax.shard_map(body, mesh=mesh, in_specs=in_specs, out_specs=out_specs, check_vma=False)
```

time: 88.1 us -> 73.5 us (0.83)
  blocking collectives: 73.9 us -> 67 us
  Pallas kernels: 12.1 us -> 5.59 us
  local copies, waits for them, and re-layouts: 1.23 us -> 0.01 us
    all_to_all x1, blocking collectives: 73.9 us -> 67 us  [body(): lax.all_to_all(packed, 'sp', split_axis=0, concat_axis=0, axis_index_grou...]
    pallas_call x2, Pallas kernels: 12.1 us -> 5.59 us  [the longest x1 4.48 us: fill(): pl.pallas_call(fill_kernel, in_specs=[hbm] * 6, out_specs=pl.BlockSpec(me...]
    broadcast_in_dim x1 -> x0, local copies, waits for them, and re-layouts: 1.23 us -> none  [body(): query = jnp.broadcast_to(new_query.reshape(1, columns), (8, columns))]
where the time goes in v2:
time: 73.5 us; the launch traced here: 73.2 us
  blocking collectives  67 us (91%)
  Pallas kernels  5.59 us (8%)
    all_to_all x1, blocking collectives, body(): lax.all_to_all(packed, 'sp', split_axis=0, concat_axis=0, axis_index_grou...  67 us
    pallas_call x1, Pallas kernels, fill(): pl.pallas_call(fill_kernel, in_specs=[hbm] * 6, out_specs=pl.BlockSpec(me...  4.48 us

profile of v2, /device:TPU:65, one launch (start us, length us, event | category | flops | bytes accessed | tf_op | source)
XLA Modules:
  0.0 73.2 jit_solution(16141197933625401351)
XLA Ops:
  0.6 0.0 copy-start
  0.6 4.5 %fill.1 = bf16[2,4,4,25,2,128]{5,4,3,2,1,0:T(2,128)(2,1)S(1)} custom-call(bf16[768,2048]{1,0:T(8,128)(2,1)} %x_hbm.1, f32[1,2048]{1,0:T(1,128)} %bitcast.9, bf16[2048,128]{1,0:T(8,128)(2,1)} %kw_hbm.1, bf16[2048,128]{1,0:T(8,128)(2,1)} %vw_hbm.1, bf16[1,128]{1,0:T(2,128)(2,1)} %bitcast.10, f32[2]{0:T(128)} %offset_hbm.1), custom_call_target="tpu_custom_call" | custom-call | tf_op jit(solution)/shard_map/fill/pallas_call | solution.py:153
  5.1 67.0 %all_to_all.5.moved_ref = bf16[32,25,2,128]{3,2,1,0:T(2,128)(2,1)S(1)} all-to-all(bf16[32,25,2,128]{3,2,1,0:T(2,128)(2,1)S(1)} %bitcast.7), channel_id=1, replica_groups={{0,64,128,192,16,80,144,208,32,96,160,224,48,112,176,240,8,72,136,200,2..., dimensions={0} | all-to-all | bytes 819200 | tf_op jit(solution)/shard_map/all_to_all | solution.py:259
  72.1 0.0 copy-done
  72.1 1.1 %settle.1 = (bf16[4,4,2,48,64]{4,3,2,1,0:T(8,128)(2,1)}, bf16[4,4,2,48,64]{4,3,2,1,0:T(8,128)(2,1)}, bf16[1,128]{1,0:T(2,128)(2,1)}) custom-call(bf16[32,25,2,128]{3,2,1,0:T(2,128)(2,1)S(1)} %all_to_all.5.moved_ref, f32[1,128]{1,0:T(1,128)S(1)} %bitcast.8), custom_call_target="tpu_custom_call" | custom-call | tf_op jit(solution)/shard_map/settle/pallas_call | solution.py:236
Async XLA Ops:
  0.6 71.5 %copy-start = (f32[128]{0:T(128)S(1)}, f32[128]{0:T(128)}, u32[]{:S(2)}) copy-start(f32[128]{0:T(128)} %param.13) | copy-start | bytes 1540

commit v3 on v2

v3 whole, which is shorter than its diff:
```python
import functools

import jax
import jax.numpy as jnp
from jax import lax
from jax.experimental import pallas as pl
from jax.experimental.pallas import tpu as pltpu
from jax.sharding import PartitionSpec as P

EPSILON = 1e-06
STEPS = 2
PARTS = 4
GROUP = 32
ORDER = [2 * (z + 4 * j) + c for c in (1, 0) for z in range(4) for j in range(4)]


def split3(value):
    high = value.astype(jnp.bfloat16).astype(jnp.float32)
    rest = value - high
    middle = rest.astype(jnp.bfloat16).astype(jnp.float32)
    return high, middle, rest - middle


def fill_kernel(
    places, x_hbm, gain_hbm, kw_hbm, vw_hbm, query_hbm, offset_hbm, out_ref,
    x_ref, w_ref, gain_ref, query_ref, offset_ref, normed_ref, head_ref, x_sem, w_sem, sem,
):
    steps, tile, _ = x_ref.shape
    columns = kw_hbm.shape[1]
    half = columns // 2
    rows = 2 * (out_ref.shape[1] - 1)
    count = steps * tile
    chunks = count // columns

    part = tile // PARTS

    def part_copy(i, p):
        return pltpu.make_async_copy(
            x_hbm.at[pl.ds(i * tile + p * part, part), :],
            x_ref.at[i, pl.ds(p * part, part), :],
            x_sem.at[i, p],
        )

    gain_copy = pltpu.make_async_copy(gain_hbm, gain_ref, sem.at[0])
    query_copy = pltpu.make_async_copy(query_hbm, query_ref, sem.at[1])
    offset_copy = pltpu.make_async_copy(offset_hbm, offset_ref, sem.at[2])
    key_copy = pltpu.make_async_copy(kw_hbm, w_ref.at[:, pl.ds(0, columns)], w_sem.at[0])
    value_copy = pltpu.make_async_copy(vw_hbm, w_ref.at[:, pl.ds(columns, columns)], w_sem.at[1])
    gain_copy.start()
    part_copy(0, 0).start()
    key_copy.start()
    value_copy.start()
    for i in range(steps):
        for p in range(PARTS):
            if i + p:
                part_copy(i, p).start(priority=1)
    query_copy.start(priority=1)
    offset_copy.start(priority=1)

    low = lax.broadcasted_iota(jnp.int32, (tile, columns), 1) < half

    tile_subs = tile // rows

    def multiply(i, carry):
        for p in range(PARTS):
            part_copy(i, p).wait()
            for r in range(p * part, (p + 1) * part, GROUP):
                x32 = x_ref[i, r : r + GROUP, :].astype(jnp.float32)
                mean_square = jnp.mean(x32 * x32, axis=-1, keepdims=True)
                scale = lax.rsqrt(mean_square + EPSILON)
                normed_ref[r : r + GROUP, :] = (x32 * scale * gain_ref[...]).astype(jnp.bfloat16)

        @pl.when(i == 0)
        def _():
            key_copy.wait()
            value_copy.wait()

        both = jnp.dot(normed_ref[...], w_ref[...], preferred_element_type=jnp.float32)
        keys, values = both[:, :columns], both[:, columns:]
        heads = [
            jnp.where(low, keys, pltpu.roll(values, half, 1)).astype(jnp.bfloat16),
            jnp.where(low, pltpu.roll(keys, half, 1), values).astype(jnp.bfloat16),
        ]
        for h in range(2):
            head_ref[h, pl.ds(i * tile, tile), :] = heads[h]
            for j in range(tile_subs):
                place = places[h][j]
                for later in range(1, steps):
                    place = jnp.where(i == later, places[h][later * tile_subs + j], place)
                out_ref[place, 0 : rows // 2] = heads[h][j * rows : (j + 1) * rows].reshape(
                    rows // 2, 2, columns
                )
        return carry

    gain_copy.wait()
    lax.fori_loop(0, steps, multiply, 0)
    query_copy.wait()
    offset_copy.wait()

    low8 = lax.broadcasted_iota(jnp.int32, (8, columns), 1) < half
    query = jnp.broadcast_to(query_ref[...].astype(jnp.float32), (8, columns))
    queries = [
        jnp.where(low8, query, 0.0).astype(jnp.bfloat16),
        jnp.where(low8, pltpu.roll(query, half, 1), 0.0).astype(jnp.bfloat16),
    ]
    upper = (
        lax.broadcasted_iota(jnp.int32, (columns, columns), 0)
        > lax.broadcasted_iota(jnp.int32, (columns, columns), 1)
    ).astype(jnp.bfloat16)
    scores = jnp.concatenate(
        [
            lax.dot_general(
                queries[h], head_ref[h], (((1,), (1,)), ((), ())), preferred_element_type=jnp.float32
            )
            * half ** (-0.5)
            + offset_ref[h]
            for h in range(2)
        ],
        axis=0,
    )
    soft = jnp.log1p(jnp.exp(-jnp.abs(scores)))
    remain = -(jnp.maximum(scores, 0.0) + soft)
    taken = jnp.minimum(scores, 0.0) - soft
    pieces = [remain[:, c * columns : (c + 1) * columns] for c in range(chunks)]
    stacked = jnp.concatenate(
        [part.astype(jnp.bfloat16) for piece in pieces for part in split3(piece)], axis=0
    )
    summed = jnp.dot(stacked, upper, preferred_element_type=jnp.float32)
    later = jnp.zeros((16, 1), jnp.float32)
    after = [None] * chunks
    for c in reversed(range(chunks)):
        base = c * 48
        within = summed[base : base + 16] + summed[base + 16 : base + 32] + summed[base + 32 : base + 48]
        after[c] = within + later
        later = later + jnp.sum(pieces[c], axis=1, keepdims=True)
    sticks = jnp.exp(taken + jnp.concatenate(after, axis=1))
    rounded = sticks.astype(jnp.bfloat16).astype(jnp.float32)
    rest = sticks - rounded
    mixed = []
    for h in range(2):
        parts = jnp.concatenate([rounded[h * 8 : h * 8 + 8], rest[h * 8 : h * 8 + 8]], axis=0)
        products = jnp.dot(
            parts.astype(jnp.bfloat16), head_ref[h], preferred_element_type=jnp.float32
        )
        mixed.append(products[0:8] + products[8:16])

    line = lax.broadcasted_iota(jnp.int32, (8, columns), 0)
    lane = lax.broadcasted_iota(jnp.int32, (8, columns), 1)
    weighted = jnp.where(low8, pltpu.roll(mixed[0], half, 1), mixed[1])
    sums = jnp.zeros((8, columns), jnp.float32)
    for at, part in enumerate(split3(later[0:8]) + split3(later[8:16])):
        sums = jnp.where(lane == at, part, sums)
    payload = jnp.where(line == 0, weighted, sums)[0:2].astype(jnp.bfloat16)
    shape = (out_ref.shape[0], 1, 2, columns)
    out_ref[:, rows // 2 :] = jnp.broadcast_to(payload, shape)


def fill(rows, norm_gain, key_weight, value_weight, query, offset, order):
    count, width = rows.shape
    columns = key_weight.shape[1]
    heads = offset.shape[0]
    subs = len(order) // heads
    places = [[order.index(h * subs + j) for j in range(subs)] for h in range(heads)]
    tile = count // STEPS
    hbm = pl.BlockSpec(memory_space=pl.ANY)
    out_shape = (len(order), count // subs // 2 + 1, 2, columns)
    return pl.pallas_call(
        functools.partial(fill_kernel, places),
        in_specs=[hbm] * 6,
        out_specs=pl.BlockSpec(memory_space=pltpu.VMEM),
        out_shape=pltpu.VMEM(out_shape, jnp.bfloat16),
        scratch_shapes=[
            pltpu.VMEM((STEPS, tile, width), jnp.bfloat16),
            pltpu.VMEM((width, 2 * columns), jnp.bfloat16),
            pltpu.VMEM((1, width), jnp.float32),
            pltpu.VMEM((1, columns), jnp.bfloat16),
            pltpu.SMEM((heads,), jnp.float32),
            pltpu.VMEM((tile, width), jnp.bfloat16),
            pltpu.VMEM((heads, count, columns), jnp.bfloat16),
            pltpu.SemaphoreType.DMA((STEPS, PARTS)),
            pltpu.SemaphoreType.DMA((2,)),
            pltpu.SemaphoreType.DMA((3,)),
        ],
        name="fill",
    )(
        rows, norm_gain.reshape(1, width), key_weight, value_weight,
        query.reshape(1, columns), offset,
    )


def settle_kernel(
    order, moved_ref, gain_ref, keys_hbm, values_hbm, read_hbm, keys_ref, values_ref, read_ref, sem
):
    peers, rows, half = keys_ref.shape
    columns = 2 * half
    key_copy = pltpu.make_async_copy(keys_ref, keys_hbm, sem.at[0])
    value_copy = pltpu.make_async_copy(values_ref, values_hbm, sem.at[1])
    for at, block in enumerate(order):
        both = moved_ref[at, 0 : rows // 2].reshape(rows, columns)
        keys_ref[block] = both[:, :half]
        values_ref[block] = both[:, half:]
    key_copy.start()
    value_copy.start()

    payload = moved_ref[:, rows // 2].astype(jnp.float32)
    weighted, sums = payload[:, 0, :], payload[:, 1, :]
    at_row = lax.broadcasted_iota(jnp.int32, (peers, 1), 0)
    at_col = lax.broadcasted_iota(jnp.int32, (1, peers), 1)
    block_row, block_col = at_row, at_col
    for at, block in enumerate(order):
        block_row = jnp.where(at_row == at, block, block_row)
        block_col = jnp.where(at_col == at, block, block_col)
    after = jnp.where(block_col > block_row, 1.0, 0.0).astype(jnp.bfloat16)
    beyond = jnp.dot(after, sums.astype(jnp.bfloat16), preferred_element_type=jnp.float32)
    lane = lax.broadcasted_iota(jnp.int32, (peers, columns), 1)
    first = jnp.sum(jnp.where(lane < 3, beyond, 0.0), axis=1, keepdims=True)
    second = jnp.sum(jnp.where((lane >= 3) & (lane < 6), beyond, 0.0), axis=1, keepdims=True)
    low = lane < half
    mixed = jnp.sum(weighted * jnp.exp(jnp.where(low, first, second)), axis=0, keepdims=True)
    low = low[0:1]
    square = mixed * mixed
    first = jnp.sum(jnp.where(low, square, 0.0), axis=1, keepdims=True) / half
    second = jnp.sum(jnp.where(low, 0.0, square), axis=1, keepdims=True) / half
    scale = lax.rsqrt(jnp.where(low, first, second) + EPSILON)
    read_ref[...] = (mixed * scale * gain_ref[...]).astype(jnp.bfloat16)
    read_copy = pltpu.make_async_copy(read_ref, read_hbm, sem.at[2])
    read_copy.start()
    key_copy.wait()
    value_copy.wait()
    read_copy.wait()


def settle(moved, gain, order):
    peers, rows, _, columns = moved.shape
    rows, half = 2 * (rows - 1), columns // 2
    cache = jax.ShapeDtypeStruct((peers, rows, half), jnp.bfloat16)
    vmem = pl.BlockSpec(memory_space=pltpu.VMEM)
    hbm = pl.BlockSpec(memory_space=pl.ANY)
    buffer = pltpu.VMEM((peers, rows, half), jnp.bfloat16)
    return pl.pallas_call(
        functools.partial(settle_kernel, order),
        in_specs=[vmem, vmem],
        out_specs=[hbm, hbm, hbm],
        out_shape=[cache, cache, jax.ShapeDtypeStruct((1, columns), jnp.bfloat16)],
        scratch_shapes=[
            buffer, buffer, pltpu.VMEM((1, columns), jnp.bfloat16), pltpu.SemaphoreType.DMA((3,)),
        ],
        name="settle",
    )(
        pltpu.with_memory_space_constraint(moved, pltpu.VMEM),
        pltpu.with_memory_space_constraint(gain.reshape(1, columns), pltpu.VMEM),
    )


def body(prompt_rows, norm_gain, key_weight, value_weight, new_query, score_offset, output_gain):
    columns = key_weight.shape[1]
    peers = lax.axis_size("sp")
    order = ORDER if len(ORDER) == peers else list(range(peers))
    packed = fill(
        prompt_rows, norm_gain, key_weight, value_weight, new_query, score_offset, order
    )
    moved = lax.all_to_all(
        packed, "sp", split_axis=0, concat_axis=0, axis_index_groups=[order], tiled=True
    )
    keys, values, first_read = settle(moved, output_gain, order)
    target = (1, 1, *keys.shape)
    return (keys.reshape(target), values.reshape(target), first_read.reshape(columns))


def solution(mesh):
    in_specs = (
        P(("grp", "sp"), None),
        P(),
        P(None, "tp"),
        P(None, "tp"),
        P(("grp", "tp")),
        P("tp"),
        P("tp"),
    )
    out_specs = (
        P(("grp", "tp"), "sp", None, None, None),
        P(("grp", "tp"), "sp", None, None, None),
        P(("grp", "tp")),
    )
    return jax.shard_map(body, mesh=mesh, in_specs=in_specs, out_specs=out_specs, check_vma=False)
```

time: 73.5 us -> 73.4 us (level)
  no operation moved by 1% of the time
where the time goes in v3:
time: 73.4 us; the launch traced here: 73 us
  blocking collectives  66.3 us (90%)
  Pallas kernels  6.07 us (8%)
    all_to_all x1, blocking collectives, body(): lax.all_to_all(packed, 'sp', split_axis=0, concat_axis=0, axis_index_grou...  66.3 us
    pallas_call x1, Pallas kernels, fill(): pl.pallas_call(functools.partial(fill_kernel, places), in_specs=[hbm] * 6...  4.89 us

profile of v3, /device:TPU:65, one launch (start us, length us, event | category | flops | bytes accessed | tf_op | source)
XLA Modules:
  0.0 73.0 jit_solution(6550844398006482186)
XLA Ops:
  0.6 0.0 copy-start
  0.6 4.9 %fill.1 = bf16[32,25,2,128]{3,2,1,0:T(2,128)(2,1)S(1)} custom-call(bf16[768,2048]{1,0:T(8,128)(2,1)} %x_hbm.1, f32[1,2048]{1,0:T(1,128)} %bitcast.7, bf16[2048,128]{1,0:T(8,128)(2,1)} %kw_hbm.1, bf16[2048,128]{1,0:T(8,128)(2,1)} %vw_hbm.1, bf16[1,128]{1,0:T(2,128)(2,1)} %bitcast.8, f32[2]{0:T(128)} %offset_hbm.1), custom_call_target="tpu_custom_call" | custom-call | tf_op jit(solution)/shard_map/fill/pallas_call | solution.py:167
  5.5 66.3 %all_to_all.5.moved_ref = bf16[32,25,2,128]{3,2,1,0:T(2,128)(2,1)S(1)} all-to-all(bf16[32,25,2,128]{3,2,1,0:T(2,128)(2,1)S(1)} %fill.1), channel_id=1, replica_groups={{8,72,136,200,24,88,152,216,40,104,168,232,56,120,184,248,0,64,128,192,..., dimensions={0} | all-to-all | bytes 819200 | tf_op jit(solution)/shard_map/all_to_all | solution.py:262
  71.8 0.0 copy-done
  71.8 1.2 %settle.1 = (bf16[32,48,64]{2,1,0:T(8,128)(2,1)}, bf16[32,48,64]{2,1,0:T(8,128)(2,1)}, bf16[1,128]{1,0:T(2,128)(2,1)}) custom-call(bf16[32,25,2,128]{3,2,1,0:T(2,128)(2,1)S(1)} %all_to_all.5.moved_ref, f32[1,128]{1,0:T(1,128)S(1)} %bitcast.6), custom_call_target="tpu_custom_call" | custom-call | tf_op jit(solution)/shard_map/settle/pallas_call | solution.py:240
Async XLA Ops:
  0.6 71.2 %copy-start = (f32[128]{0:T(128)S(1)}, f32[128]{0:T(128)}, u32[]{:S(2)}) copy-start(f32[128]{0:T(128)} %param.13) | copy-start | bytes 1540

commit v4 on v3

--- a/solution.py
+++ b/solution.py
@@ -9,8 +9,8 @@
 
 EPSILON = 1e-06
 STEPS = 2
-PARTS = 4
-GROUP = 32
+PARTS = 1
+GROUP = 128
 ORDER = [2 * (z + 4 * j) + c for c in (1, 0) for z in range(4) for j in range(4)]
 
 
@@ -47,9 +47,9 @@
     key_copy = pltpu.make_async_copy(kw_hbm, w_ref.at[:, pl.ds(0, columns)], w_sem.at[0])
     value_copy = pltpu.make_async_copy(vw_hbm, w_ref.at[:, pl.ds(columns, columns)], w_sem.at[1])
     gain_copy.start()
-    part_copy(0, 0).start()
     key_copy.start()
     value_copy.start()
+    part_copy(0, 0).start()
     for i in range(steps):
         for p in range(PARTS):
             if i + p:
@@ -69,11 +69,6 @@
                 mean_square = jnp.mean(x32 * x32, axis=-1, keepdims=True)
                 scale = lax.rsqrt(mean_square + EPSILON)
                 normed_ref[r : r + GROUP, :] = (x32 * scale * gain_ref[...]).astype(jnp.bfloat16)
-
-        @pl.when(i == 0)
-        def _():
-            key_copy.wait()
-            value_copy.wait()
 
         both = jnp.dot(normed_ref[...], w_ref[...], preferred_element_type=jnp.float32)
         keys, values = both[:, :columns], both[:, columns:]
@@ -93,6 +88,8 @@
         return carry
 
     gain_copy.wait()
+    key_copy.wait()
+    value_copy.wait()
     lax.fori_loop(0, steps, multiply, 0)
     query_copy.wait()
     offset_copy.wait()

time: 73.4 us -> 72.9 us (level)
  no operation moved by 1% of the time
where the time goes in v4:
time: 72.9 us; the launch traced here: 72.5 us
  blocking collectives  66.3 us (91%)
  Pallas kernels  5.56 us (8%)
    all_to_all x1, blocking collectives, body(): lax.all_to_all(packed, 'sp', split_axis=0, concat_axis=0, axis_index_grou...  66.3 us
    pallas_call x1, Pallas kernels, fill(): pl.pallas_call(functools.partial(fill_kernel, places), in_specs=[hbm] * 6...  4.39 us

profile of v4, /device:TPU:65, one launch (start us, length us, event | category | flops | bytes accessed | tf_op | source)
XLA Modules:
  0.0 72.5 jit_solution(13864942186765887640)
XLA Ops:
  0.6 0.0 copy-start
  0.6 4.4 %fill.1 = bf16[32,25,2,128]{3,2,1,0:T(2,128)(2,1)S(1)} custom-call(bf16[768,2048]{1,0:T(8,128)(2,1)} %x_hbm.1, f32[1,2048]{1,0:T(1,128)} %bitcast.7, bf16[2048,128]{1,0:T(8,128)(2,1)} %kw_hbm.1, bf16[2048,128]{1,0:T(8,128)(2,1)} %vw_hbm.1, bf16[1,128]{1,0:T(2,128)(2,1)} %bitcast.8, f32[2]{0:T(128)} %offset_hbm.1), custom_call_target="tpu_custom_call" | custom-call | tf_op jit(solution)/shard_map/fill/pallas_call | solution.py:164
  5.0 66.3 %all_to_all.5.moved_ref = bf16[32,25,2,128]{3,2,1,0:T(2,128)(2,1)S(1)} all-to-all(bf16[32,25,2,128]{3,2,1,0:T(2,128)(2,1)S(1)} %fill.1), channel_id=1, replica_groups={{8,72,136,200,24,88,152,216,40,104,168,232,56,120,184,248,0,64,128,192,..., dimensions={0} | all-to-all | bytes 819200 | tf_op jit(solution)/shard_map/all_to_all | solution.py:259
  71.3 0.0 copy-done
  71.3 1.2 %settle.1 = (bf16[32,48,64]{2,1,0:T(8,128)(2,1)}, bf16[32,48,64]{2,1,0:T(8,128)(2,1)}, bf16[1,128]{1,0:T(2,128)(2,1)}) custom-call(bf16[32,25,2,128]{3,2,1,0:T(2,128)(2,1)S(1)} %all_to_all.5.moved_ref, f32[1,128]{1,0:T(1,128)S(1)} %bitcast.6), custom_call_target="tpu_custom_call" | custom-call | tf_op jit(solution)/shard_map/settle/pallas_call | solution.py:237
Async XLA Ops:
  0.6 70.7 %copy-start = (f32[128]{0:T(128)S(1)}, f32[128]{0:T(128)}, u32[]{:S(2)}) copy-start(f32[128]{0:T(128)} %param.13) | copy-start | bytes 1540
